TPU v7x, 32 devices: a whole 2x2x4 slice. The times are simulated.
32 devices in a mesh: grp: 2 (over y), sp: 4 (over z), tp: 4 (over x, core).
Axes of the slice: x: 2, y: 2, z: 4, core: 2. Of those that a mesh axis runs over, the one named last changes fastest.
Arguments:
- tokens_in: bfloat16 [2048, 2048], P(('grp', 'sp'), 'tp'), parts along dimension 0, may hold values from -6 to 6
- norm_gain: float32 [3, 2048], replicated, may hold values from 0.1 to 1.9
- w_pool_in: bfloat16 [3, 2048, 1024], P(None, 'sp', 'tp'), may hold values from -0.125 to 0.125
- w_gate: bfloat16 [3, 2048, 2048], P(None, 'sp', 'tp'), may hold values from -0.125 to 0.125
- w_back: bfloat16 [3, 1024, 2048], P(None, 'tp', 'sp'), may hold values from -0.25 to 0.25
Outputs:
- tokens_out: bfloat16 [2048, 2048], P(('grp', 'sp'), 'tp'), parts along dimension 0
There are 2 independent parts, one for each index of `grp`. A program takes and returns all parts, laid end to end along the dimension named above; an argument that names none is the same for every part. Nothing has to cross between parts.
All inputs are finite; a program needn't handle non-finite values.
Results may differ from a plain program's by a relative error of at most 0.017.
Values may be sent and summed in bfloat16 or wider, within the bound.
A program may use at most 64 MiB of HBM per device.

v0:
```python
import jax
import jax.numpy as jnp
from jax import lax
from jax.sharding import PartitionSpec as P

POOL_WIDTH = 1024
GROUPS = 4
GRID_W = 32
LAYERS = 3
pool_windows = (2, 4, 8, 16)
norm_eps = 1e-06


def padded_2(value, sides, width):
    for axis, dim in sides:
        peers, length = (lax.axis_size(axis), value.shape[dim])
        up = [(i, (i + 1) % peers) for i in range(peers - 1)]
        down = [(j, i) for i, j in up]
        last = lax.slice_in_dim(value, length - width, length, axis=dim)
        initial = lax.slice_in_dim(value, 0, width, axis=dim)
        before = lax.ppermute(last, axis, up)
        after = lax.ppermute(initial, axis, down)
        value = jnp.concatenate([before, value, after], axis=dim)
    return value


def window_means(padded, rows_here, first_row, total_rows, window):
    reach = max(pool_windows) // 2
    half_span = window // 2
    width_cols = padded.shape[1] - 2 * reach
    row_sums = padded[reach - half_span : reach - half_span + rows_here]
    for offset in range(1 - half_span, half_span):
        row_sums = row_sums + padded[reach + offset : reach + offset + rows_here]
    box_sums = row_sums[:, reach - half_span : reach - half_span + width_cols]
    for offset in range(1 - half_span, half_span):
        box_sums = box_sums + row_sums[:, reach + offset : reach + offset + width_cols]
    row_index = first_row + jnp.arange(rows_here, dtype=jnp.int32)
    col_index = jnp.arange(width_cols, dtype=jnp.int32)
    row_counts = jnp.minimum(row_index + half_span, total_rows) - jnp.maximum(
        row_index - half_span, 0
    )
    col_counts = jnp.minimum(col_index + half_span, width_cols) - jnp.maximum(
        col_index - half_span, 0
    )
    counts = (row_counts[:, None] * col_counts[None, :]).astype(jnp.float32)
    return box_sums / counts[:, :, None]


def on_device(tokens_in, norm_gain, w_pool_in, w_gate, w_back):
    reach = max(pool_windows) // 2
    sp_count = lax.axis_size("sp")
    tp_count = lax.axis_size("tp")
    tp_pos = lax.axis_index("tp")
    sp_pos = lax.axis_index("sp")
    tok_rows = tokens_in.shape[0]
    rows_here = tok_rows // GRID_W
    total_rows = rows_here * sp_count
    first_row = sp_pos * rows_here
    local_pool = w_pool_in.shape[2]
    group_width = POOL_WIDTH // GROUPS
    channel_group = (tp_pos * local_pool + jnp.arange(local_pool, dtype=jnp.int32)) // group_width
    state = tokens_in
    for layer_id in range(LAYERS):
        whole_rows = lax.all_gather(state, "tp", axis=1, tiled=True)
        wide = whole_rows.astype(jnp.float32)
        normed = (
            wide
            * lax.rsqrt(jnp.mean(wide * wide, axis=-1, keepdims=True) + norm_eps)
            * norm_gain[layer_id]
        ).astype(jnp.bfloat16)
        pool_acc = jnp.dot(
            normed,
            lax.all_gather(w_pool_in[layer_id], "sp", axis=0, tiled=True),
            preferred_element_type=jnp.float32,
        )
        gate_acc = jnp.dot(
            normed,
            lax.all_gather(w_gate[layer_id], "sp", axis=0, tiled=True),
            preferred_element_type=jnp.float32,
        )
        pool_in = pool_acc.astype(jnp.bfloat16)
        gate = jax.nn.sigmoid(gate_acc)
        cells = pool_in.reshape(rows_here, GRID_W, local_pool)
        rimmed = padded_2(cells, (("sp", 0),), reach)
        padded = jnp.pad(rimmed.astype(jnp.float32), ((0, 0), (reach, reach), (0, 0)))
        means = jnp.zeros((rows_here, GRID_W, local_pool), jnp.float32)
        for group_id in range(GROUPS):
            in_group = (channel_group == group_id)[None, None, :]
            means = jnp.where(
                in_group,
                window_means(padded, rows_here, first_row, total_rows, pool_windows[group_id]),
                means,
            )
        pooled = (
            (means - cells.astype(jnp.float32)).reshape(tok_rows, local_pool).astype(jnp.bfloat16)
        )
        full_pooled = lax.all_gather(pooled, "tp", axis=1, tiled=True)
        back_rows = lax.all_gather(w_back[layer_id], "sp", axis=1, tiled=True)
        back_cols = lax.all_to_all(back_rows, "tp", split_axis=1, concat_axis=0, tiled=True)
        partials = jnp.einsum(
            "tnb,nbd->ntd",
            full_pooled.reshape(tok_rows, tp_count, local_pool),
            back_cols.reshape(tp_count, local_pool, back_cols.shape[1]),
            preferred_element_type=jnp.float32,
        ).astype(jnp.bfloat16)
        branch = jnp.sum(partials.astype(jnp.float32), axis=0)
        state = (state.astype(jnp.float32) + gate * branch).astype(jnp.bfloat16)
    return state


def solution(mesh):
    return jax.shard_map(
        on_device,
        mesh=mesh,
        in_specs=(
            P(("grp", "sp"), "tp"),
            P(),
            P(None, "sp", "tp"),
            P(None, "sp", "tp"),
            P(None, "tp", "sp"),
        ),
        out_specs=P(("grp", "sp"), "tp"),
        check_vma=False,
    )
```

profile of v0, /device:TPU:0, one launch (start us, length us, event | category | flops | bytes accessed | tf_op | source)
XLA Modules:
  0.0 391.0 jit_solution(7945444731493379469)
XLA Ops:
  13.5 14.9 %all-gather.22.cloned.1.call-done = bf16[256,2048]{1,0:T(8,128)(2,1)} async-done(((bf16[256,512]{1,0:T(8,128)(2,1)}), bf16[256,2048]{1,0:T(8,128)(2,1)}) %all-gather.22.cloned.1.call-update) | async-done | bytes 1048592 | tf_op jit(solution)/shard_map/all_gather | solution.py:64
  29.9 28.1 %all-gather.30.cloned.1.call-done = bf16[1,2048,256]{2,1,0:T(8,128)(2,1)} async-done(((bf16[1,512,256]{2,1,0:T(8,128)(2,1)}), bf16[1,2048,256]{2,1,0:T(8,128)(2,1)}) %all-gather.30.cloned.1.call-update) | async-done | bytes 1048592 | tf_op jit(solution)/shard_map/all_gather | solution.py:73
  60.0 3.4 collective-permute-start
  64.7 23.0 %all-gather.32.cloned.1.call-done = bf16[1,256,2048]{1,2,0:T(8,128)(2,1)} async-done(((bf16[1,256,512]{1,2,0:T(8,128)(2,1)}), bf16[1,256,2048]{1,2,0:T(8,128)(2,1)}) %all-gather.32.cloned.1.call-update) | async-done | bytes 1048592 | tf_op jit(solution)/shard_map/all_gather | solution.py:98
  90.0 3.5 all-to-all-start
  94.9 16.6 %all_gather.48 = bf16[256,1024]{1,0:T(8,128)(2,1)S(1)} all-gather(bf16[256,256]{1,0:T(8,128)(2,1)S(1)} %bitcast.112), channel_id=1, replica_groups=mesh['grp'=2,'sp'=4,'tp'=4] {'tp'}, dimensions={1}, use_global_device_ids=true | all-gather | bytes 655360 | tf_op jit(solution)/shard_map/all_gather | solution.py:97
  112.3 21.1 %all-gather.28.cloned.1.call-done = bf16[1,2048,512]{2,1,0:T(8,128)(2,1)} async-done(((bf16[1,512,512]{2,1,0:T(8,128)(2,1)}), bf16[1,2048,512]{2,1,0:T(8,128)(2,1)}) %all-gather.28.cloned.1.call-update) | async-done | bytes 2097168 | tf_op jit(solution)/shard_map/all_gather | solution.py:78
  133.4 3.2 fusion.75
  138.8 13.4 %all-gather.24.cloned.1.call-done = bf16[256,2048]{1,0:T(8,128)(2,1)} async-done(((bf16[256,512]{1,0:T(8,128)(2,1)}), bf16[256,2048]{1,0:T(8,128)(2,1)}) %all-gather.24.cloned.1.call-update) | async-done | bytes 1048592 | tf_op jit(solution)/shard_map/all_gather | solution.py:64
  153.8 27.9 %all-gather.36.cloned.1.call-done = bf16[1,2048,256]{2,1,0:T(8,128)(2,1)} async-done(((bf16[1,512,256]{2,1,0:T(8,128)(2,1)}), bf16[1,2048,256]{2,1,0:T(8,128)(2,1)}) %all-gather.36.cloned.1.call-update) | async-done | bytes 1048592 | tf_op jit(solution)/shard_map/all_gather | solution.py:73
  183.7 3.4 collective-permute-start.2
  188.4 23.1 %all-gather.38.cloned.1.call-done = bf16[1,256,2048]{1,2,0:T(8,128)(2,1)} async-done(((bf16[1,256,512]{1,2,0:T(8,128)(2,1)}), bf16[1,256,2048]{1,2,0:T(8,128)(2,1)}) %all-gather.38.cloned.1.call-update) | async-done | bytes 1048592 | tf_op jit(solution)/shard_map/all_gather | solution.py:98
  213.7 3.5 all-to-all-start.1
  219.2 16.1 %all_gather.53 = bf16[256,1024]{1,0:T(8,128)(2,1)S(1)} all-gather(bf16[256,256]{1,0:T(8,128)(2,1)S(1)} %bitcast.113), channel_id=1, replica_groups=mesh['grp'=2,'sp'=4,'tp'=4] {'tp'}, dimensions={1}, use_global_device_ids=true | all-gather | bytes 655360 | tf_op jit(solution)/shard_map/all_gather | solution.py:97
  236.0 21.2 %all-gather.34.cloned.1.call-done = bf16[1,2048,512]{2,1,0:T(8,128)(2,1)} async-done(((bf16[1,512,512]{2,1,0:T(8,128)(2,1)}), bf16[1,2048,512]{2,1,0:T(8,128)(2,1)}) %all-gather.34.cloned.1.call-update) | async-done | bytes 2097168 | tf_op jit(solution)/shard_map/all_gather | solution.py:78
  257.3 3.1 fusion.72
  262.5 13.6 %all-gather.26.cloned.1.call-done = bf16[256,2048]{1,0:T(8,128)(2,1)} async-done(((bf16[256,512]{1,0:T(8,128)(2,1)}), bf16[256,2048]{1,0:T(8,128)(2,1)}) %all-gather.26.cloned.1.call-update) | async-done | bytes 1048592 | tf_op jit(solution)/shard_map/all_gather | solution.py:64
  277.6 27.9 %all-gather.42.cloned.1.call-done = bf16[1,2048,256]{2,1,0:T(8,128)(2,1)} async-done(((bf16[1,512,256]{2,1,0:T(8,128)(2,1)}), bf16[1,2048,256]{2,1,0:T(8,128)(2,1)}) %all-gather.42.cloned.1.call-update) | async-done | bytes 1048592 | tf_op jit(solution)/shard_map/all_gather | solution.py:73
  307.6 3.4 collective-permute-start.4
  312.2 23.1 %all-gather.44.cloned.1.call-done = bf16[1,256,2048]{1,2,0:T(8,128)(2,1)} async-done(((bf16[1,256,512]{1,2,0:T(8,128)(2,1)}), bf16[1,256,2048]{1,2,0:T(8,128)(2,1)}) %all-gather.44.cloned.1.call-update) | async-done | bytes 1048592 | tf_op jit(solution)/shard_map/all_gather | solution.py:98
  337.6 3.7 all-to-all-start.2
  343.1 16.1 %all_gather.58 = bf16[256,1024]{1,0:T(8,128)(2,1)S(1)} all-gather(bf16[256,256]{1,0:T(8,128)(2,1)S(1)} %bitcast.111), channel_id=1, replica_groups=mesh['grp'=2,'sp'=4,'tp'=4] {'tp'}, dimensions={1}, use_global_device_ids=true | all-gather | bytes 655360 | tf_op jit(solution)/shard_map/all_gather | solution.py:97
  359.9 21.1 %all-gather.40.cloned.1.call-done = bf16[1,2048,512]{2,1,0:T(8,128)(2,1)} async-done(((bf16[1,512,512]{2,1,0:T(8,128)(2,1)}), bf16[1,2048,512]{2,1,0:T(8,128)(2,1)}) %all-gather.40.cloned.1.call-update) | async-done | bytes 2097168 | tf_op jit(solution)/shard_map/all_gather | solution.py:78
  381.0 3.1 fusion.69
  (137 shorter events, 39.5 us)
Async XLA Ops:
  6.5 21.8 %all-gather.22.cloned.1.call-start = ((), (), s32[]{:S(2)}) async-start(), calls=%async_computation.3 | async-start | bytes 1310720 | tf_op jit(solution)/shard_map/all_gather | solution.py:64
  7.3 50.7 %all-gather.30.cloned.1.call-start = ((), (), s32[]{:S(2)}) async-start(), calls=%async_computation.7 | async-start | bytes 1310720 | tf_op jit(solution)/shard_map/all_gather | solution.py:73
  9.5 78.2 %all-gather.32.cloned.1.call-start = ((), (), s32[]{:S(2)}) async-start(), calls=%async_computation.8 | async-start | bytes 1310720 | tf_op jit(solution)/shard_map/all_gather | solution.py:98
  11.2 122.2 %all-gather.28.cloned.1.call-start = ((), (), s32[]{:S(2)}) async-start(), calls=%async_computation.6 | async-start | bytes 2621440 | tf_op jit(solution)/shard_map/all_gather | solution.py:78
  13.5 46.5 %copy-start.10 = (f32[1,2048]{1,0:T(1,128)}, f32[1,2048]{1,0:T(1,128)S(1)}, u32[]{:S(2)}) copy-start(f32[1,2048]{1,0:T(1,128)S(1)} %get-tuple-element.27) | copy-start | bytes 24580
  29.9 60.1 %copy-start.23 = (f32[256]{0:T(256)}, f32[256]{0:T(256)S(1)}, u32[]{:S(2)}) copy-start(f32[256]{0:T(256)S(1)} %add_rsqrt_fusion.2) | copy-start | bytes 3076
  60.0 33.6 %collective-permute-start = (bf16[8,32,256]{2,1,0:T(8,128)(2,1)S(1)}, bf16[8,32,256]{2,1,0:T(8,128)(2,1)S(1)}, u32[]{:S(2)}, u32[]{:S(2)}) collective-permute-start(bf16[8,32,256]{2,1,0:T(8,128)(2,1)S(1)} %bitcast.99), channel_id=1, source_target_pairs={{0,4},{4,8},{8,12},{1,5},{5,9},{9,13},{2,6},{6,10},{10,14},{3,7},{... | collective-permute-start | bytes 393224 | tf_op jit(solution)/shard_map/ppermute | solution.py:21
  63.3 30.2 %collective-permute-start.1 = (bf16[8,32,256]{2,1,0:T(8,128)(2,1)S(1)}, bf16[8,32,256]{2,1,0:T(8,128)(2,1)S(1)}, u32[]{:S(2)}, u32[]{:S(2)}) collective-permute-start(bf16[8,32,256]{2,1,0:T(8,128)(2,1)S(1)} %bitcast.100), channel_id=1, source_target_pairs={{4,0},{8,4},{12,8},{5,1},{9,5},{13,9},{6,2},{10,6},{14,10},{7,3},{... | collective-permute-start | bytes 393224 | tf_op jit(solution)/shard_map/ppermute | solution.py:22
  90.0 21.8 %all-to-all-start = ((bf16[256,4,512]{2,0,1:T(8,128)(2,1)}), bf16[256,4,512]{2,0,1:T(8,128)(2,1)S(1)}, u32[]{:S(2)}, u32[]{:S(2)}) async-start(bf16[256,4,512]{2,0,1:T(8,128)(2,1)} %copy.20), calls=%async_computation | async-start | bytes 2097152 | tf_op jit(solution)/shard_map/all_to_all | solution.py:99
  93.5 58.7 %all-gather.24.cloned.1.call-start = ((), (), s32[]{:S(2)}) async-start(), calls=%async_computation.4 | async-start | bytes 1310720 | tf_op jit(solution)/shard_map/all_gather | solution.py:64
  136.6 45.1 %all-gather.36.cloned.1.call-start = ((), (), s32[]{:S(2)}) async-start(), calls=%async_computation.10 | async-start | bytes 1310720 | tf_op jit(solution)/shard_map/all_gather | solution.py:73
  137.1 74.3 %all-gather.38.cloned.1.call-start = ((), (), s32[]{:S(2)}) async-start(), calls=%async_computation.11 | async-start | bytes 1310720 | tf_op jit(solution)/shard_map/all_gather | solution.py:98
  138.1 119.2 %all-gather.34.cloned.1.call-start = ((), (), s32[]{:S(2)}) async-start(), calls=%async_computation.9 | async-start | bytes 2621440 | tf_op jit(solution)/shard_map/all_gather | solution.py:78
  153.8 60.0 %copy-start.24 = (f32[256]{0:T(256)}, f32[256]{0:T(256)S(1)}, u32[]{:S(2)}) copy-start(f32[256]{0:T(256)S(1)} %add_rsqrt_fusion.1) | copy-start | bytes 3076
  183.7 33.6 %collective-permute-start.2 = (bf16[8,32,256]{2,1,0:T(8,128)(2,1)S(1)}, bf16[8,32,256]{2,1,0:T(8,128)(2,1)S(1)}, u32[]{:S(2)}, u32[]{:S(2)}) collective-permute-start(bf16[8,32,256]{2,1,0:T(8,128)(2,1)S(1)} %bitcast.107), channel_id=1, source_target_pairs={{0,4},{4,8},{8,12},{1,5},{5,9},{9,13},{2,6},{6,10},{10,14},{3,7},{... | collective-permute-start | bytes 393224 | tf_op jit(solution)/shard_map/ppermute | solution.py:21
  187.1 30.3 %collective-permute-start.3 = (bf16[8,32,256]{2,1,0:T(8,128)(2,1)S(1)}, bf16[8,32,256]{2,1,0:T(8,128)(2,1)S(1)}, u32[]{:S(2)}, u32[]{:S(2)}) collective-permute-start(bf16[8,32,256]{2,1,0:T(8,128)(2,1)S(1)} %bitcast.108), channel_id=1, source_target_pairs={{4,0},{8,4},{12,8},{5,1},{9,5},{13,9},{6,2},{10,6},{14,10},{7,3},{... | collective-permute-start | bytes 393224 | tf_op jit(solution)/shard_map/ppermute | solution.py:22
  213.7 21.8 %all-to-all-start.1 = ((bf16[256,4,512]{2,0,1:T(8,128)(2,1)}), bf16[256,4,512]{2,0,1:T(8,128)(2,1)S(1)}, u32[]{:S(2)}, u32[]{:S(2)}) async-start(bf16[256,4,512]{2,0,1:T(8,128)(2,1)} %copy.24), calls=%async_computation.1 | async-start | bytes 2097152 | tf_op jit(solution)/shard_map/all_to_all | solution.py:99
  217.3 58.8 %all-gather.26.cloned.1.call-start = ((), (), s32[]{:S(2)}) async-start(), calls=%async_computation.5 | async-start | bytes 1310720 | tf_op jit(solution)/shard_map/all_gather | solution.py:64
  260.4 45.1 %all-gather.42.cloned.1.call-start = ((), (), s32[]{:S(2)}) async-start(), calls=%async_computation.13 | async-start | bytes 1310720 | tf_op jit(solution)/shard_map/all_gather | solution.py:73
  261.0 74.3 %all-gather.44.cloned.1.call-start = ((), (), s32[]{:S(2)}) async-start(), calls=%async_computation.14 | async-start | bytes 1310720 | tf_op jit(solution)/shard_map/all_gather | solution.py:98
  261.9 119.0 %all-gather.40.cloned.1.call-start = ((), (), s32[]{:S(2)}) async-start(), calls=%async_computation.12 | async-start | bytes 2621440 | tf_op jit(solution)/shard_map/all_gather | solution.py:78
  307.6 33.7 %collective-permute-start.4 = (bf16[8,32,256]{2,1,0:T(8,128)(2,1)S(1)}, bf16[8,32,256]{2,1,0:T(8,128)(2,1)S(1)}, u32[]{:S(2)}, u32[]{:S(2)}) collective-permute-start(bf16[8,32,256]{2,1,0:T(8,128)(2,1)S(1)} %bitcast.103), channel_id=1, source_target_pairs={{0,4},{4,8},{8,12},{1,5},{5,9},{9,13},{2,6},{6,10},{10,14},{3,7},{... | collective-permute-start | bytes 393224 | tf_op jit(solution)/shard_map/ppermute | solution.py:21
  310.9 30.4 %collective-permute-start.5 = (bf16[8,32,256]{2,1,0:T(8,128)(2,1)S(1)}, bf16[8,32,256]{2,1,0:T(8,128)(2,1)S(1)}, u32[]{:S(2)}, u32[]{:S(2)}) collective-permute-start(bf16[8,32,256]{2,1,0:T(8,128)(2,1)S(1)} %bitcast.104), channel_id=1, source_target_pairs={{4,0},{8,4},{12,8},{5,1},{9,5},{13,9},{6,2},{10,6},{14,10},{7,3},{... | collective-permute-start | bytes 393224 | tf_op jit(solution)/shard_map/ppermute | solution.py:22
  337.6 21.8 %all-to-all-start.2 = ((bf16[256,4,512]{2,0,1:T(8,128)(2,1)}), bf16[256,4,512]{2,0,1:T(8,128)(2,1)S(1)}, u32[]{:S(2)}, u32[]{:S(2)}) async-start(bf16[256,4,512]{2,0,1:T(8,128)(2,1)} %copy.28), calls=%async_computation.2 | async-start | bytes 2097152 | tf_op jit(solution)/shard_map/all_to_all | solution.py:99
  (23 other events, 437.2 us)
Sparse Core Ops, SparseCore 0:
  8.9 19.4 all-gather.21
  29.9 27.9 all-gather.29
  59.5 28.1 all-gather.31
  89.1 44.1 all-gather.27
  136.7 15.4 all-gather.23
  153.7 27.9 all-gather.35
  183.2 28.1 all-gather.37
  213.0 44.1 all-gather.33
  260.6 15.4 all-gather.25
  277.5 27.9 all-gather.41
  307.1 28.1 all-gather.43
  336.7 44.2 all-gather.39
where the time goes:
time: 392 us; the launch traced here: 391 us
  waiting for transfers between devices  261 us (67%)
  blocking collectives  48.8 us (12%)
  starting transfers between devices  25.1 us (6%)
  matrix products  16.9 us (4%)
  local copies, waits for them, and re-layouts  15.8 us (4%)
  between operations  14.2 us (4%)
  other arithmetic  8.76 us (2%)
    all_gather x3, waiting for transfers between devices, on_device(): lax.all_gather(w_pool_in[layer_id], 'sp', axis=0, tiled=True)  83.9 us
    all_gather x3, waiting for transfers between devices, on_device(): back_rows = lax.all_gather(w_back[layer_id], 'sp', axis=1, tiled=True)  69.2 us
    all_gather x3, waiting for transfers between devices, on_device(): lax.all_gather(w_gate[layer_id], 'sp', axis=0, tiled=True)  63.4 us
    all_gather x3, blocking collectives, on_device(): full_pooled = lax.all_gather(pooled, 'tp', axis=1, tiled=True)  48.8 us
    all_gather x3, waiting for transfers between devices, on_device(): whole_rows = lax.all_gather(state, 'tp', axis=1, tiled=True)  41.8 us
    all_to_all x3, starting transfers between devices, on_device(): lax.all_to_all(back_rows, 'tp', split_axis=1, concat_axis=0, tiled=True)  10.7 us
    ppermute x3, starting transfers between devices, padded_2(): before = lax.ppermute(last, axis, up)  10.1 us
    dot_general x3, matrix products, on_device(): jnp.dot(normed, lax.all_gather(w_gate[layer_id], 'sp', axis=0, tiled=True...  9.41 us
  transfers between devices with their start and end apart: 21, of which 12 were waited for; matrix products, arithmetic and copies ran while one was open for 8% of the time, Pallas kernels for 0%

commit v1 on v0

--- a/solution.py
+++ b/solution.py
@@ -9,6 +9,17 @@
 LAYERS = 3
 pool_windows = (2, 4, 8, 16)
 norm_eps = 1e-06
+
+
+def turned_line(x, axis, d):
+    n_dev = lax.axis_size(axis)
+    right = [(i, (i + 1) % n_dev) for i in range(n_dev)]
+    parts = [x]
+    for far in range(1, n_dev):
+        parts = [lax.ppermute(parts[0], axis, right), *parts]
+    whole = jnp.concatenate(parts, axis=d)
+    places = (lax.axis_index(axis) + 1) * parts[-1].shape[d]
+    return jnp.roll(whole, places, axis=d)
 
 
 def padded_2(value, sides, width):
@@ -95,7 +106,7 @@
             (means - cells.astype(jnp.float32)).reshape(tok_rows, local_pool).astype(jnp.bfloat16)
         )
         full_pooled = lax.all_gather(pooled, "tp", axis=1, tiled=True)
-        back_rows = lax.all_gather(w_back[layer_id], "sp", axis=1, tiled=True)
+        back_rows = turned_line(w_back[layer_id], "sp", 1)
         back_cols = lax.all_to_all(back_rows, "tp", split_axis=1, concat_axis=0, tiled=True)
         partials = jnp.einsum(
             "tnb,nbd->ntd",

time: 392 us -> 315 us (0.80)
  waiting for transfers between devices: 261 us -> 166 us
  other arithmetic: 8.76 us -> 31.9 us
  local copies, waits for them, and re-layouts: 15.8 us -> 10.9 us
    all_gather x3 -> x0, waiting for transfers between devices: 69.2 us -> none  [on_device(): back_rows = lax.all_gather(w_back[layer_id], 'sp', axis=1, tiled=True)]
    ppermute x0 -> x9, waiting for transfers between devices: none -> 41.2 us  [turned_line(): parts = [lax.ppermute(parts[0], axis, right), *parts]]
    all_gather x3, waiting for transfers between devices: 63.4 us -> 25.9 us  [on_device(): lax.all_gather(w_gate[layer_id], 'sp', axis=0, tiled=True)]
    all_gather x3, waiting for transfers between devices: 41.8 us -> 13.9 us  [on_device(): whole_rows = lax.all_gather(state, 'tp', axis=1, tiled=True)]
    concatenate x0 -> x2, other arithmetic: none -> 22 us  [turned_line(): return jnp.roll(whole, places, axis=d)]
    ppermute x0 -> x9, starting transfers between devices: none -> 4.99 us  [turned_line(): parts = [lax.ppermute(parts[0], axis, right), *parts]]
    all_gather x3, waiting for transfers between devices: 83.9 us -> 78.9 us  [on_device(): lax.all_gather(w_pool_in[layer_id], 'sp', axis=0, tiled=True)]
  transfers between devices with their start and end apart: 21 -> 27, of which waited for: 12 -> 14; matrix products, arithmetic and copies ran while one was open for 8% -> 16% of each run, Pallas kernels for 0% -> 0%
where the time goes in v1:
time: 315 us; the launch traced here: 314 us
  waiting for transfers between devices  166 us (53%)
  blocking collectives  45.2 us (14%)
  other arithmetic  31.9 us (10%)
  starting transfers between devices  29 us (9%)
  matrix products  17.3 us (5%)
  between operations  13.8 us (4%)
  local copies, waits for them, and re-layouts  10.9 us (3%)
    all_gather x3, waiting for transfers between devices, on_device(): lax.all_gather(w_pool_in[layer_id], 'sp', axis=0, tiled=True)  78.9 us
    all_gather x3, blocking collectives, on_device(): full_pooled = lax.all_gather(pooled, 'tp', axis=1, tiled=True)  45.2 us
    ppermute x9, waiting for transfers between devices, turned_line(): parts = [lax.ppermute(parts[0], axis, right), *parts]  41.2 us
    all_gather x3, waiting for transfers between devices, on_device(): lax.all_gather(w_gate[layer_id], 'sp', axis=0, tiled=True)  25.9 us
    concatenate x2, other arithmetic, turned_line(): return jnp.roll(whole, places, axis=d)  22 us
    all_gather x3, waiting for transfers between devices, on_device(): whole_rows = lax.all_gather(state, 'tp', axis=1, tiled=True)  13.9 us
    all_to_all x3, starting transfers between devices, on_device(): lax.all_to_all(back_rows, 'tp', split_axis=1, concat_axis=0, tiled=True)  10.5 us
    dot_general x3, matrix products, on_device(): jnp.dot(normed, lax.all_gather(w_gate[layer_id], 'sp', axis=0, tiled=True...  9.73 us
  transfers between devices with their start and end apart: 27, of which 14 were waited for; matrix products, arithmetic and copies ran while one was open for 16% of the time, Pallas kernels for 0%

profile of v1, /device:TPU:0, one launch (start us, length us, event | category | flops | bytes accessed | tf_op | source)
XLA Modules:
  0.0 314.0 jit_solution(10059739187569393528)
XLA Ops:
  15.6 6.1 %collective-permute-done.2 = bf16[256,512]{0,1:T(8,128)(2,1)S(1)} collective-permute-done((bf16[256,512]{0,1:T(8,128)(2,1)S(1)}, bf16[256,512]{0,1:T(8,128)(2,1)S(1)}, u32[]{:S(2)}, u32[]{:S(2)}) %collective-permute-start.2) | collective-permute-done | bytes 262176 | tf_op jit(solution)/shard_map/ppermute | solution.py:19
  21.9 9.1 %collective-permute-done.3 = bf16[256,512]{0,1:T(8,128)(2,1)S(1)} collective-permute-done((bf16[256,512]{0,1:T(8,128)(2,1)S(1)}, bf16[256,512]{0,1:T(8,128)(2,1)S(1)}, u32[]{:S(2)}, u32[]{:S(2)}) %collective-permute-start.3) | collective-permute-done | bytes 262176 | tf_op jit(solution)/shard_map/ppermute | solution.py:19
  32.5 25.4 %all-gather.24.cloned.1.call-done = bf16[1,2048,256]{2,1,0:T(8,128)(2,1)} async-done(((bf16[1,512,256]{2,1,0:T(8,128)(2,1)}), bf16[1,2048,256]{2,1,0:T(8,128)(2,1)}) %all-gather.24.cloned.1.call-update) | async-done | bytes 1048592 | tf_op jit(solution)/shard_map/all_gather | solution.py:84
  60.0 3.4 %collective-permute-start = (bf16[8,32,256]{2,1,0:T(8,128)(2,1)S(1)}, bf16[8,32,256]{2,1,0:T(8,128)(2,1)S(1)}, u32[]{:S(2)}, u32[]{:S(2)}) collective-permute-start(bf16[8,32,256]{2,1,0:T(8,128)(2,1)S(1)} %bitcast.112), channel_id=1, source_target_pairs={{0,4},{4,8},{8,12},{1,5},{5,9},{9,13},{2,6},{6,10},{10,14},{3,7},{... | collective-permute-start | bytes 393224 | tf_op jit(solution)/shard_map/ppermute | solution.py:32
  64.6 9.6 %fusion.96 = bf16[256,2048]{0,1:T(8,128)(2,1)S(1)} fusion(s32[]{:T(128)S(6)} %select_n.83, bf16[256,512]{0,1:T(8,128)(2,1)S(1)} %collective-permute-done.4, bf16[256,512]{0,1:T(8,128)(2,1)S(1)} %collective-permute-done.3, bf16[256,512]{0,1:T(8,128)(2,1)S(1)} %collective-permute-done.2, bf16[256,512]{0,1:T(8,128)(2,1)S(1)} %bitcast.103), kind=kLoop, calls=%fused_computation.95 | loop fusion | flops 8388608 | bytes 2097156 | tf_op jit(solution)/shard_map/jit(_roll_dynamic)/concatenate | solution.py:22
  75.6 3.5 %all-to-all-start = ((bf16[256,4,512]{2,0,1:T(8,128)(2,1)}), bf16[256,4,512]{2,0,1:T(8,128)(2,1)S(1)}, u32[]{:S(2)}, u32[]{:S(2)}) async-start(bf16[256,4,512]{2,0,1:T(8,128)(2,1)} %copy.20), calls=%async_computation | async-start | bytes 2097152 | tf_op jit(solution)/shard_map/all_to_all | solution.py:110
  80.6 16.6 %all_gather.39 = bf16[256,1024]{1,0:T(8,128)(2,1)S(1)} all-gather(bf16[256,256]{1,0:T(8,128)(2,1)S(1)} %bitcast.121), channel_id=1, replica_groups=mesh['grp'=2,'sp'=4,'tp'=4] {'tp'}, dimensions={1}, use_global_device_ids=true | all-gather | bytes 655360 | tf_op jit(solution)/shard_map/all_gather | solution.py:108
  97.9 6.7 %all-gather.22.cloned.1.call-done = bf16[1,2048,512]{2,1,0:T(8,128)(2,1)} async-done(((bf16[1,512,512]{2,1,0:T(8,128)(2,1)}), bf16[1,2048,512]{2,1,0:T(8,128)(2,1)}) %all-gather.22.cloned.1.call-update) | async-done | bytes 2097168 | tf_op jit(solution)/shard_map/all_gather | solution.py:89
  110.6 9.0 %collective-permute-done.12 = bf16[256,512]{0,1:T(8,128)(2,1)S(1)} collective-permute-done((bf16[256,512]{0,1:T(8,128)(2,1)S(1)}, bf16[256,512]{0,1:T(8,128)(2,1)S(1)}, u32[]{:S(2)}, u32[]{:S(2)}) %collective-permute-start.12) | collective-permute-done | bytes 262176 | tf_op jit(solution)/shard_map/ppermute | solution.py:19
  119.6 5.6 %collective-permute-done.7 = bf16[256,512]{0,1:T(8,128)(2,1)S(1)} collective-permute-done((bf16[256,512]{0,1:T(8,128)(2,1)S(1)}, bf16[256,512]{0,1:T(8,128)(2,1)S(1)}, u32[]{:S(2)}, u32[]{:S(2)}) %collective-permute-start.7) | collective-permute-done | bytes 262176 | tf_op jit(solution)/shard_map/ppermute | solution.py:19
  125.2 5.6 %collective-permute-done.13 = bf16[256,512]{0,1:T(8,128)(2,1)S(1)} collective-permute-done((bf16[256,512]{0,1:T(8,128)(2,1)S(1)}, bf16[256,512]{0,1:T(8,128)(2,1)S(1)}, u32[]{:S(2)}, u32[]{:S(2)}) %collective-permute-start.13) | collective-permute-done | bytes 262176 | tf_op jit(solution)/shard_map/ppermute | solution.py:19
  130.8 5.7 %collective-permute-done.8 = bf16[256,512]{0,1:T(8,128)(2,1)S(1)} collective-permute-done((bf16[256,512]{0,1:T(8,128)(2,1)S(1)}, bf16[256,512]{0,1:T(8,128)(2,1)S(1)}, u32[]{:S(2)}, u32[]{:S(2)}) %collective-permute-start.8) | collective-permute-done | bytes 262176 | tf_op jit(solution)/shard_map/ppermute | solution.py:19
  138.2 25.4 %all-gather.28.cloned.1.call-done = bf16[1,2048,256]{2,1,0:T(8,128)(2,1)} async-done(((bf16[1,512,256]{2,1,0:T(8,128)(2,1)}), bf16[1,2048,256]{2,1,0:T(8,128)(2,1)}) %all-gather.28.cloned.1.call-update) | async-done | bytes 1048592 | tf_op jit(solution)/shard_map/all_gather | solution.py:84
  170.3 12.4 %fusion.82 = (bf16[256,2048]{0,1:T(8,128)(2,1)S(1)}, bf16[256,2048]{0,1:T(8,128)(2,1)S(1)}) fusion(s32[]{:T(128)S(6)} %select_n.83, bf16[256,512]{0,1:T(8,128)(2,1)} %copy-done.6, bf16[256,512]{0,1:T(8,128)(2,1)S(1)} %collective-permute-done.13, bf16[256,512]{0,1:T(8,128)(2,1)S(1)} %collective-permute-done.12, bf16[256,512]{0,1:T(8,128)(2,1)S(1)} %bitcast.105, ...), kind=kLoop, calls=%fused_computation.81 | loop fusion | flops 16777216 | bytes 4194308 | tf_op jit(solution)/shard_map/jit(_roll_dynamic)/concatenate | solution.py:22
  184.0 3.5 %all-to-all-start.1 = ((bf16[256,4,512]{2,0,1:T(8,128)(2,1)}), bf16[256,4,512]{2,0,1:T(8,128)(2,1)S(1)}, u32[]{:S(2)}, u32[]{:S(2)}) async-start(bf16[256,4,512]{2,0,1:T(8,128)(2,1)} %copy.24), calls=%async_computation.1 | async-start | bytes 2097152 | tf_op jit(solution)/shard_map/all_to_all | solution.py:110
  190.5 15.1 %all_gather.43 = bf16[256,1024]{1,0:T(8,128)(2,1)S(1)} all-gather(bf16[256,256]{1,0:T(8,128)(2,1)S(1)} %bitcast.122), channel_id=1, replica_groups=mesh['grp'=2,'sp'=4,'tp'=4] {'tp'}, dimensions={1}, use_global_device_ids=true | all-gather | bytes 655360 | tf_op jit(solution)/shard_map/all_gather | solution.py:108
  209.2 3.5 %fusion.72 = bf16[256,512]{1,0:T(8,128)(2,1)} fusion(f32[256,512]{1,0:T(8,128)S(1)} %convert_reduce_fusion.1, bf16[1,2048,512]{2,1,0:T(8,128)(2,1)} %all-gather.26.cloned.1.call-done, bf16[256,512]{1,0:T(8,128)(2,1)S(1)} %copy-done.7, bf16[256,2048]{1,0:T(8,128)(2,1)} %all-gather.18.cloned.1.call-done, f32[2048]{0:T(1024)S(1)} %bitcast.126, ...), kind=kOutput, calls=%fused_computation.72 | convolution fusion | flops 539885568 | bytes 4203520 | tf_op jit(solution)/shard_map/dot_general | solution.py:87
  214.2 13.9 %all-gather.20.cloned.1.call-done = bf16[256,2048]{1,0:T(8,128)(2,1)} async-done(((bf16[256,512]{1,0:T(8,128)(2,1)}), bf16[256,2048]{1,0:T(8,128)(2,1)}) %all-gather.20.cloned.1.call-update) | async-done | bytes 1048592 | tf_op jit(solution)/shard_map/all_gather | solution.py:75
  229.6 28.1 %all-gather.32.cloned.1.call-done = bf16[1,2048,256]{2,1,0:T(8,128)(2,1)} async-done(((bf16[1,512,256]{2,1,0:T(8,128)(2,1)}), bf16[1,2048,256]{2,1,0:T(8,128)(2,1)}) %all-gather.32.cloned.1.call-update) | async-done | bytes 1048592 | tf_op jit(solution)/shard_map/all_gather | solution.py:84
  259.7 3.4 %collective-permute-start.10 = (bf16[8,32,256]{2,1,0:T(8,128)(2,1)S(1)}, bf16[8,32,256]{2,1,0:T(8,128)(2,1)S(1)}, u32[]{:S(2)}, u32[]{:S(2)}) collective-permute-start(bf16[8,32,256]{2,1,0:T(8,128)(2,1)S(1)} %bitcast.116), channel_id=1, source_target_pairs={{0,4},{4,8},{8,12},{1,5},{5,9},{9,13},{2,6},{6,10},{10,14},{3,7},{... | collective-permute-start | bytes 393224 | tf_op jit(solution)/shard_map/ppermute | solution.py:32
  265.7 3.5 %all-to-all-start.2 = ((bf16[256,4,512]{2,0,1:T(8,128)(2,1)}), bf16[256,4,512]{2,0,1:T(8,128)(2,1)S(1)}, u32[]{:S(2)}, u32[]{:S(2)}) async-start(bf16[256,4,512]{2,0,1:T(8,128)(2,1)} %copy.28), calls=%async_computation.2 | async-start | bytes 2097152 | tf_op jit(solution)/shard_map/all_to_all | solution.py:110
  269.2 3.3 %collective-permute-done.11 = bf16[8,32,256]{2,1,0:T(8,128)(2,1)S(1)} collective-permute-done((bf16[8,32,256]{2,1,0:T(8,128)(2,1)S(1)}, bf16[8,32,256]{2,1,0:T(8,128)(2,1)S(1)}, u32[]{:S(2)}, u32[]{:S(2)}) %collective-permute-start.11) | collective-permute-done | bytes 131104 | tf_op jit(solution)/shard_map/ppermute | solution.py:33
  273.9 13.4 %all_gather.47 = bf16[256,1024]{1,0:T(8,128)(2,1)S(1)} all-gather(bf16[256,256]{1,0:T(8,128)(2,1)S(1)} %bitcast.120), channel_id=1, replica_groups=mesh['grp'=2,'sp'=4,'tp'=4] {'tp'}, dimensions={1}, use_global_device_ids=true | all-gather | bytes 655360 | tf_op jit(solution)/shard_map/all_gather | solution.py:108
  288.0 16.3 %all-gather.30.cloned.1.call-done = bf16[1,2048,512]{2,1,0:T(8,128)(2,1)} async-done(((bf16[1,512,512]{2,1,0:T(8,128)(2,1)}), bf16[1,2048,512]{2,1,0:T(8,128)(2,1)}) %all-gather.30.cloned.1.call-update) | async-done | bytes 2097168 | tf_op jit(solution)/shard_map/all_gather | solution.py:89
  (140 shorter events, 51.9 us)
Async XLA Ops:
  6.5 24.5 %all-gather.16.cloned.1.call-start = ((), (), s32[]{:S(2)}) async-start(), calls=%async_computation.3 | async-start | bytes 1310720 | tf_op jit(solution)/shard_map/all_gather | solution.py:75
  7.3 50.7 %all-gather.24.cloned.1.call-start = ((), (), s32[]{:S(2)}) async-start(), calls=%async_computation.7 | async-start | bytes 1310720 | tf_op jit(solution)/shard_map/all_gather | solution.py:84
  9.3 95.2 %all-gather.22.cloned.1.call-start = ((), (), s32[]{:S(2)}) async-start(), calls=%async_computation.6 | async-start | bytes 2621440 | tf_op jit(solution)/shard_map/all_gather | solution.py:89
  10.3 11.4 %collective-permute-start.2 = (bf16[256,512]{0,1:T(8,128)(2,1)S(1)}, bf16[256,512]{0,1:T(8,128)(2,1)S(1)}, u32[]{:S(2)}, u32[]{:S(2)}) collective-permute-start(bf16[256,512]{0,1:T(8,128)(2,1)S(1)} %bitcast.102), channel_id=1, source_target_pairs={{0,4},{4,8},{8,12},{12,0},{1,5},{5,9},{9,13},{13,1},{2,6},{6,10},{... | collective-permute-start | bytes 786440 | tf_op jit(solution)/shard_map/ppermute | solution.py:19
  31.0 33.6 %collective-permute-start.4 = (bf16[256,512]{0,1:T(8,128)(2,1)S(1)}, bf16[256,512]{0,1:T(8,128)(2,1)S(1)}, u32[]{:S(2)}, u32[]{:S(2)}) collective-permute-start(bf16[256,512]{0,1:T(8,128)(2,1)S(1)} %collective-permute-done.3), channel_id=1, source_target_pairs={{0,4},{4,8},{8,12},{12,0},{1,5},{5,9},{9,13},{13,1},{2,6},{6,10},{... | collective-permute-start | bytes 786440 | tf_op jit(solution)/shard_map/ppermute | solution.py:19
  60.0 19.2 %collective-permute-start = (bf16[8,32,256]{2,1,0:T(8,128)(2,1)S(1)}, bf16[8,32,256]{2,1,0:T(8,128)(2,1)S(1)}, u32[]{:S(2)}, u32[]{:S(2)}) collective-permute-start(bf16[8,32,256]{2,1,0:T(8,128)(2,1)S(1)} %bitcast.112), channel_id=1, source_target_pairs={{0,4},{4,8},{8,12},{1,5},{5,9},{9,13},{2,6},{6,10},{10,14},{3,7},{... | collective-permute-start | bytes 393224 | tf_op jit(solution)/shard_map/ppermute | solution.py:32
  63.3 15.9 %collective-permute-start.1 = (bf16[8,32,256]{2,1,0:T(8,128)(2,1)S(1)}, bf16[8,32,256]{2,1,0:T(8,128)(2,1)S(1)}, u32[]{:S(2)}, u32[]{:S(2)}) collective-permute-start(bf16[8,32,256]{2,1,0:T(8,128)(2,1)S(1)} %bitcast.113), channel_id=1, source_target_pairs={{4,0},{8,4},{12,8},{5,1},{9,5},{13,9},{6,2},{10,6},{14,10},{7,3},{... | collective-permute-start | bytes 393224 | tf_op jit(solution)/shard_map/ppermute | solution.py:33
  75.6 21.8 %all-to-all-start = ((bf16[256,4,512]{2,0,1:T(8,128)(2,1)}), bf16[256,4,512]{2,0,1:T(8,128)(2,1)S(1)}, u32[]{:S(2)}, u32[]{:S(2)}) async-start(bf16[256,4,512]{2,0,1:T(8,128)(2,1)} %copy.20), calls=%async_computation | async-start | bytes 2097152 | tf_op jit(solution)/shard_map/all_to_all | solution.py:110
  79.1 57.4 %all-gather.18.cloned.1.call-start = ((), (), s32[]{:S(2)}) async-start(), calls=%async_computation.4 | async-start | bytes 1310720 | tf_op jit(solution)/shard_map/all_gather | solution.py:75
  107.8 55.9 %all-gather.28.cloned.1.call-start = ((), (), s32[]{:S(2)}) async-start(), calls=%async_computation.9 | async-start | bytes 1310720 | tf_op jit(solution)/shard_map/all_gather | solution.py:84
  108.3 100.9 %all-gather.26.cloned.1.call-start = ((), (), s32[]{:S(2)}) async-start(), calls=%async_computation.8 | async-start | bytes 2621440 | tf_op jit(solution)/shard_map/all_gather | solution.py:89
  108.5 11.0 %collective-permute-start.12 = (bf16[256,512]{0,1:T(8,128)(2,1)S(1)}, bf16[256,512]{0,1:T(8,128)(2,1)S(1)}, u32[]{:S(2)}, u32[]{:S(2)}) collective-permute-start(bf16[256,512]{0,1:T(8,128)(2,1)S(1)} %bitcast.104), channel_id=1, source_target_pairs={{0,4},{4,8},{8,12},{12,0},{1,5},{5,9},{9,13},{13,1},{2,6},{6,10},{... | collective-permute-start | bytes 786440 | tf_op jit(solution)/shard_map/ppermute | solution.py:19
  108.9 16.3 %collective-permute-start.7 = (bf16[256,512]{0,1:T(8,128)(2,1)S(1)}, bf16[256,512]{0,1:T(8,128)(2,1)S(1)}, u32[]{:S(2)}, u32[]{:S(2)}) collective-permute-start(bf16[256,512]{0,1:T(8,128)(2,1)S(1)} %bitcast.106), channel_id=1, source_target_pairs={{0,4},{4,8},{8,12},{12,0},{1,5},{5,9},{9,13},{13,1},{2,6},{6,10},{... | collective-permute-start | bytes 786440 | tf_op jit(solution)/shard_map/ppermute | solution.py:19
  119.6 11.2 %collective-permute-start.13 = (bf16[256,512]{0,1:T(8,128)(2,1)S(1)}, bf16[256,512]{0,1:T(8,128)(2,1)S(1)}, u32[]{:S(2)}, u32[]{:S(2)}) collective-permute-start(bf16[256,512]{0,1:T(8,128)(2,1)S(1)} %collective-permute-done.12), channel_id=1, source_target_pairs={{0,4},{4,8},{8,12},{12,0},{1,5},{5,9},{9,13},{13,1},{2,6},{6,10},{... | collective-permute-start | bytes 786440 | tf_op jit(solution)/shard_map/ppermute | solution.py:19
  125.2 11.4 %collective-permute-start.8 = (bf16[256,512]{0,1:T(8,128)(2,1)S(1)}, bf16[256,512]{0,1:T(8,128)(2,1)S(1)}, u32[]{:S(2)}, u32[]{:S(2)}) collective-permute-start(bf16[256,512]{0,1:T(8,128)(2,1)S(1)} %collective-permute-done.7), channel_id=1, source_target_pairs={{0,4},{4,8},{8,12},{12,0},{1,5},{5,9},{9,13},{13,1},{2,6},{6,10},{... | collective-permute-start | bytes 786440 | tf_op jit(solution)/shard_map/ppermute | solution.py:19
  130.8 38.7 %collective-permute-start.14 = (bf16[256,512]{0,1:T(8,128)(2,1)S(1)}, bf16[256,512]{0,1:T(8,128)(2,1)S(1)}, u32[]{:S(2)}, u32[]{:S(2)}) collective-permute-start(bf16[256,512]{0,1:T(8,128)(2,1)S(1)} %collective-permute-done.13), channel_id=1, source_target_pairs={{0,4},{4,8},{8,12},{12,0},{1,5},{5,9},{9,13},{13,1},{2,6},{6,10},{... | collective-permute-start | bytes 786440 | tf_op jit(solution)/shard_map/ppermute | solution.py:19
  136.6 33.7 %collective-permute-start.9 = (bf16[256,512]{0,1:T(8,128)(2,1)S(1)}, bf16[256,512]{0,1:T(8,128)(2,1)}, u32[]{:S(2)}, u32[]{:S(2)}) collective-permute-start(bf16[256,512]{0,1:T(8,128)(2,1)S(1)} %collective-permute-done.8), channel_id=1, source_target_pairs={{0,4},{4,8},{8,12},{12,0},{1,5},{5,9},{9,13},{13,1},{2,6},{6,10},{... | collective-permute-start | bytes 786440 | tf_op jit(solution)/shard_map/ppermute | solution.py:19
  165.7 21.9 %collective-permute-start.5 = (bf16[8,32,256]{2,1,0:T(8,128)(2,1)S(1)}, bf16[8,32,256]{2,1,0:T(8,128)(2,1)}, u32[]{:S(2)}, u32[]{:S(2)}) collective-permute-start(bf16[8,32,256]{2,1,0:T(8,128)(2,1)S(1)} %bitcast.108), channel_id=1, source_target_pairs={{0,4},{4,8},{8,12},{1,5},{5,9},{9,13},{2,6},{6,10},{10,14},{3,7},{... | collective-permute-start | bytes 393224 | tf_op jit(solution)/shard_map/ppermute | solution.py:32
  168.2 19.4 %collective-permute-start.6 = (bf16[8,32,256]{2,1,0:T(8,128)(2,1)S(1)}, bf16[8,32,256]{2,1,0:T(8,128)(2,1)}, u32[]{:S(2)}, u32[]{:S(2)}) collective-permute-start(bf16[8,32,256]{2,1,0:T(8,128)(2,1)S(1)} %bitcast.109), channel_id=1, source_target_pairs={{4,0},{8,4},{12,8},{5,1},{9,5},{13,9},{6,2},{10,6},{14,10},{7,3},{... | collective-permute-start | bytes 393224 | tf_op jit(solution)/shard_map/ppermute | solution.py:33
  184.0 21.8 %all-to-all-start.1 = ((bf16[256,4,512]{2,0,1:T(8,128)(2,1)}), bf16[256,4,512]{2,0,1:T(8,128)(2,1)S(1)}, u32[]{:S(2)}, u32[]{:S(2)}) async-start(bf16[256,4,512]{2,0,1:T(8,128)(2,1)} %copy.24), calls=%async_computation.1 | async-start | bytes 2097152 | tf_op jit(solution)/shard_map/all_to_all | solution.py:110
  187.6 40.5 %all-gather.20.cloned.1.call-start = ((), (), s32[]{:S(2)}) async-start(), calls=%async_computation.5 | async-start | bytes 1310720 | tf_op jit(solution)/shard_map/all_gather | solution.py:75
  212.7 45.0 %all-gather.32.cloned.1.call-start = ((), (), s32[]{:S(2)}) async-start(), calls=%async_computation.11 | async-start | bytes 1310720 | tf_op jit(solution)/shard_map/all_gather | solution.py:84
  213.5 90.9 %all-gather.30.cloned.1.call-start = ((), (), s32[]{:S(2)}) async-start(), calls=%async_computation.10 | async-start | bytes 2621440 | tf_op jit(solution)/shard_map/all_gather | solution.py:89
  265.7 21.8 %all-to-all-start.2 = ((bf16[256,4,512]{2,0,1:T(8,128)(2,1)}), bf16[256,4,512]{2,0,1:T(8,128)(2,1)S(1)}, u32[]{:S(2)}, u32[]{:S(2)}) async-start(bf16[256,4,512]{2,0,1:T(8,128)(2,1)} %copy.28), calls=%async_computation.2 | async-start | bytes 2097152 | tf_op jit(solution)/shard_map/all_to_all | solution.py:110
  (26 other events, 607.1 us)
Sparse Core Ops, SparseCore 0:
  8.9 19.4 all-gather.15
  29.9 27.9 all-gather.23
  59.5 45.0 all-gather.21
  107.9 15.4 all-gather.17
  124.8 38.7 all-gather.27
  165.0 44.1 all-gather.25
  212.8 15.2 all-gather.19
  229.7 27.9 all-gather.31
  259.3 45.0 all-gather.29
